TPU v7x, 512 devices: a whole 4x8x8 slice. The times are simulated.
512 devices in a mesh: sp: 32 (over z, x), tp: 16 (over y, core).
Axes of the slice: x: 4, y: 8, z: 8, core: 2. Of those that a mesh axis runs over, the one named last changes fastest.
Arguments:
- stream_in: bfloat16 [8192, 2048], P(('sp', 'tp')), may hold values from -6 to 6
- queries: bfloat16 [8192, 4096], P('sp', 'tp'), may hold values from -6 to 6
- key_rows: bfloat16 [8192, 4096], P('sp', 'tp'), may hold values from -6 to 6
- values: bfloat16 [8192, 8192], P('sp', 'tp'), may hold values from -6 to 6
- decay_low: bfloat16 [8192, 16], P('sp'), may hold values from -4 to 4
- decay_matrix: bfloat16 [16, 4096], P(None, 'tp'), may hold values from -1.5 to 1.5
- decay_bias: float32 [4096], P('tp')
- decay_shift: float32 [8192, 16], P('sp', 'tp'), may hold values from -1 to 0
- head_gain: float32 [512], replicated, may hold values from 0.1 to 1.9
- output_matrix: bfloat16 [8192, 2048], P('tp'), may hold values from -0.0625 to 0.0625
- feed_gain: float32 [2048], replicated, may hold values from 0.1 to 1.9
- routes: int32 [8192, 2], P('sp'), may hold values from 0 to 31, all different within a row; in each aligned block of 256 rows (0 to 255, 256 to 511, ...) at most 16 rows name the same one
- route_weights: float32 [8192, 2], P('sp'), may hold values from 0.2 to 1
- expert_gate: bfloat16 [32, 2048, 2816], P('sp', None, 'tp'), may hold values from -0.125 to 0.125
- specialist_widen: bfloat16 [32, 2048, 2816], P('sp', None, 'tp'), may hold values from -0.125 to 0.125
- expert_down: bfloat16 [32, 2816, 2048], P('sp', 'tp'), may hold values from -0.109375 to 0.109375
Outputs:
- layer_out: bfloat16 [8192, 2048], P(('sp', 'tp'))
Inputs may be any that keep to these rules, and one draw needn't show every extreme that they name: `routes`: each row names 2 different experts; within each aligned block of 256 rows no expert is named by more than 16 rows, and in every draw some expert is named by exactly 16 rows of some block.
All inputs are finite; a program needn't handle non-finite values.
Results may differ from a plain program's by a relative error of at most 0.02.
Values may be sent and summed in bfloat16 or wider, within the bound.
A program may use at most 64 MiB of HBM per device.

v0:
```python
import jax
import jax.numpy as jnp
from jax import lax
from jax.sharding import Mesh
from jax.sharding import PartitionSpec as P

HK = 256
HV = 512
TOP = 2
BLK = 128
SP = ("sp_0", "sp_1")
TP = ("tp_0", "tp_1")
SP_TP = ("sp_0", "sp_1", "tp_0", "tp_1")
TEMPER = 16.0
EPSILON = 1e-06
HIGHEST = lax.Precision.HIGHEST


def filled_with(shard, identity):
    return jax.tree.map(
        lambda part, zero: jnp.zeros_like(part) + jnp.asarray(zero, part.dtype), shard, identity
    )


def carried_in(shard, axes, combine, identity):
    before = start = filled_with(shard, identity)
    so_far = shard
    for axis in reversed(axes):
        peers, here = (lax.axis_size(axis), lax.axis_index(axis))
        pieces = jax.tree.map(
            lambda part, kind: lax.all_gather(part.astype(kind), axis),
            so_far,
            (jnp.bfloat16, jnp.bfloat16),
        )
        inside, so_far = (start, start)
        for k in range(peers):
            passed = k < here
            so_far = combine(
                so_far, jax.tree.map(lambda part, own: part[k].astype(own.dtype), pieces, shard)
            )
            inside = jax.tree.map(lambda new, old: jnp.where(passed, new, old), so_far, inside)
        before = combine(inside, before)
    return before


def cut_along(shard, dim, peers):
    before, after = (shard.shape[:dim], shard.shape[dim + 1 :])
    return jnp.moveaxis(shard.reshape(*before, peers, -1, *after), dim, 0)


def sent_and_summed(shard, axis, dim):
    tiles = cut_along(shard, dim, lax.axis_size(axis))
    arrived = lax.all_to_all(tiles, axis, split_axis=0, concat_axis=0, tiled=True)
    return arrived.astype(jnp.float32).sum(axis=0)


def gathered_by_axis(shard, axes, dim):
    for axis in reversed(axes):
        shard = lax.all_gather(shard, axis, axis=dim, tiled=True)
    return shard


def decay_logs(decay_low, decay_matrix, decay_bias, decay_shift, heads):
    before_gate = jnp.dot(decay_low, decay_matrix, preferred_element_type=jnp.float32) + decay_bias
    logged = jax.nn.log_sigmoid(before_gate) / TEMPER
    return logged.reshape(before_gate.shape[0], heads, HK) + decay_shift[:, :, None]


def into_blocks(array):
    length, heads, width = array.shape
    return array.reshape(length // BLK, BLK, heads, width).transpose(2, 0, 1, 3)


def segment_summands(queries, key_rows, values, log_decay):
    inside = jnp.cumsum(log_decay, axis=2)
    final_position = inside[:, :, -1:, :]
    scaled_query = queries * jnp.exp(inside) * HK ** (-0.5)
    scaled_key = key_rows * jnp.exp(-inside)
    end_keys = key_rows * jnp.exp(final_position - inside)
    scores = jnp.einsum("hnid,hnjd->hnij", scaled_query, scaled_key, precision=HIGHEST)
    causal = jnp.tril(jnp.ones((BLK, BLK), jnp.bool_))
    scores = jnp.where(causal, scores, 0.0)
    local_out = jnp.einsum("hnij,hnjv->hniv", scores, values, precision=HIGHEST)
    partial_update = jnp.einsum("hnjd,hnjv->hndv", end_keys, values, precision=HIGHEST)
    return (scaled_query, local_out, partial_update, jnp.exp(final_position[:, :, 0, :]))


def run_blocks(scaled_query, partial_update, block_decay, start):

    def advance(state, pieces):
        query_block, added, decay = pieces
        output = jnp.einsum("hid,hdv->hiv", query_block, state, precision=HIGHEST)
        return (state * decay[:, :, None] + added, output)

    final, outputs = lax.scan(
        advance,
        start,
        (
            jnp.moveaxis(scaled_query, 1, 0),
            jnp.moveaxis(partial_update, 1, 0),
            jnp.moveaxis(block_decay, 1, 0),
        ),
    )
    return (final, jnp.moveaxis(outputs, 0, 1))


def link_states(earlier, later):
    return (earlier[0] * later[0], earlier[1] * later[0][..., None] + later[1])


def pass_state(device_decay, local_state):
    identity = (jnp.ones_like(device_decay), jnp.zeros_like(local_state))
    _, carried = carried_in((device_decay, local_state), SP, link_states, identity)
    return carried


def head_norm(heads_out, head_gain):
    heads = heads_out.shape[0]
    flat = heads_out.transpose(1, 2, 0, 3).reshape(-1, heads, HV)
    normed = flat * lax.rsqrt(jnp.mean(flat * flat, axis=-1, keepdims=True) + EPSILON) * head_gain
    return normed.reshape(-1, heads * HV).astype(jnp.bfloat16)


def root_scale(midstream, gain):
    return (
        midstream
        * lax.rsqrt(jnp.mean(midstream * midstream, axis=-1, keepdims=True) + EPSILON)
        * gain
    ).astype(jnp.bfloat16)


def body(
    stream_in,
    queries,
    key_rows,
    values,
    decay_low,
    decay_matrix,
    decay_bias,
    decay_shift,
    head_gain,
    output_matrix,
    feed_gain,
    routes,
    route_weights,
    expert_gate,
    specialist_widen,
    expert_down,
):
    length = queries.shape[0]
    heads = queries.shape[1] // HK
    sequence_devices = lax.axis_size(SP)
    head_devices = lax.axis_size(TP)
    width = stream_in.shape[1]
    log_decay = decay_logs(decay_low, decay_matrix, decay_bias, decay_shift, heads)

    def shaped(array, channels):
        return into_blocks(array.astype(jnp.float32).reshape(length, heads, channels))

    scaled_query, local_out, partial_update, block_decay = segment_summands(
        shaped(queries, HK), shaped(key_rows, HK), shaped(values, HV), into_blocks(log_decay)
    )
    start = jnp.zeros((heads, HK, HV), jnp.float32)
    device_decay = jnp.prod(block_decay, axis=1)
    local_state, carried_out = run_blocks(scaled_query, partial_update, block_decay, start)
    carried = pass_state(device_decay, local_state)
    shifted = jnp.concatenate([jnp.ones_like(block_decay[:, :1]), block_decay[:, :-1]], axis=1)
    before = jnp.cumprod(shifted, axis=1)
    readout = jnp.einsum(
        "hnid,hdv->hniv", scaled_query * before[:, :, None, :], carried, precision=HIGHEST
    )
    total_out = local_out + carried_out + readout
    mixed = head_norm(total_out, head_gain)
    rows_here = length // head_devices
    attended = sent_and_summed(
        jnp.dot(mixed, output_matrix, preferred_element_type=jnp.float32).astype(jnp.bfloat16),
        TP,
        0,
    )
    midstream = stream_in.astype(jnp.float32) + attended
    normed = root_scale(midstream, feed_gain)
    group = lax.all_gather(normed, TP, axis=0, tiled=True)
    experts = sequence_devices * expert_gate.shape[0]
    capacity = head_devices * max(1, TOP * length // (sequence_devices * head_devices))
    block_slots = capacity // head_devices
    own_index = lax.axis_index(TP)
    flat_routes = routes.reshape(-1)
    expert_index = jnp.arange(experts, dtype=jnp.int32)
    matches = (flat_routes[:, None] == expert_index[None, :]).astype(jnp.int32)
    ranking = jnp.sum((jnp.cumsum(matches, axis=0) - matches) * matches, axis=1)
    slot_member = (ranking[:, None] - 0 == jnp.arange(capacity, dtype=jnp.int32)[None, :]).astype(
        jnp.float32
    )
    table = slot_member[:, :, None] * matches[:, None, :].astype(jnp.float32)
    full_table = table.reshape(length, TOP, capacity * experts)
    selector = jnp.sum(full_table, axis=1).T.astype(jnp.bfloat16)
    filled = jnp.dot(selector, group, preferred_element_type=jnp.float32)
    arrived = lax.all_to_all(
        filled.astype(jnp.bfloat16).reshape(capacity, experts, width),
        SP,
        split_axis=1,
        concat_axis=1,
        tiled=True,
    )
    rows_in = arrived.reshape(-1, width)
    gated = jnp.dot(rows_in, expert_gate[0], preferred_element_type=jnp.float32)
    lifted = jnp.dot(rows_in, specialist_widen[0], preferred_element_type=jnp.float32)
    hidden = (jax.nn.silu(gated) * lifted).astype(jnp.bfloat16)
    summed = sent_and_summed(
        jnp.dot(hidden, expert_down[0], preferred_element_type=jnp.float32).astype(jnp.bfloat16),
        TP,
        0,
    )
    expert_token_rows = summed.astype(jnp.bfloat16).reshape(block_slots, sequence_devices, width)
    returned = lax.all_to_all(expert_token_rows, SP, split_axis=1, concat_axis=1, tiled=True)
    weight_table = jnp.sum(full_table * route_weights.reshape(length, TOP, 1), axis=1)
    own_weights = lax.dynamic_slice_in_dim(weight_table, own_index * rows_here, rows_here, 0)
    piece = gathered_by_axis(returned, TP, 0)
    count = piece.shape[0]
    flat_piece = piece.reshape(count * experts, width).astype(jnp.float32)
    routed = jnp.dot(own_weights, flat_piece, precision=HIGHEST, preferred_element_type=jnp.float32)
    return (midstream + routed).astype(jnp.bfloat16)


def solution(mesh):
    finer = Mesh(mesh.devices.reshape(8, 4, 8, 2), ("sp_0", "sp_1", "tp_0", "tp_1"))
    in_specs = (
        P(SP_TP, None),
        P(SP, TP),
        P(SP, TP),
        P(SP, TP),
        P(SP, None),
        P(None, TP),
        P(TP),
        P(SP, TP),
        P(),
        P(TP, None),
        P(),
        P(SP, None),
        P(SP, None),
        P(SP, None, TP),
        P(SP, None, TP),
        P(SP, TP, None),
    )
    out_specs = P(SP_TP, None)
    return jax.shard_map(body, mesh=finer, in_specs=in_specs, out_specs=out_specs, check_vma=False)
```

profile of v0, /device:TPU:2, one launch (start us, length us, event | category | flops | bytes accessed | tf_op | source)
XLA Modules:
  0.0 369.7 jit_solution(5884363078821731961)
XLA Ops:
  6.5 1.3 fusion.71
  7.8 0.3 reduce_window_sum.28
  8.1 0.9 convert_element_type.550
  9.1 2.6 convolution_bitcast_fusion.1
  11.7 4.6 %while.13 = (s32[]{:T(128)}, f32[1,256,512]{2,1,0:T(8,128)S(1)}, f32[2,1,128,512]{3,2,1,0:T(8,128)}, f32[2,1,256]{2,1,0:T(1,128)S(1)}, f32[2,1,256,512]{3,2,1,0:...) while((s32[]{:T(128)}, f32[1,256,512]{2,1,0:T(8,128)S(1)}, ...), condition=%wide.region_2.3_spmd.clone, body=%wide.region_1.2_spmd.clone.sunk | while | flops 201850880 | bytes 2494568 | solution.py:95
  11.7 1.2 fusion.144
  12.8 1.2 bitcast_add_fusion.2
  14.0 1.1 fusion.144
  15.2 1.2 bitcast_add_fusion.2
  16.3 0.7 convert_element_type.561
  17.2 12.9 %all-gather.2 = bf16[4,1,256]{2,1,0:T(2,128)(2,1)S(1)} all-gather(bf16[1,1,256]{2,1,0:T(2,128)(2,1)S(1)} %reshape.1207), channel_id=2, replica_groups=mesh['sp_0'=8,'sp_1'=4,'tp_0'=8,'tp_1'=2] {'sp_1'}, dimensions={0}, use_global_device_ids=true | all-gather | bytes 2560 | tf_op jit(solution)/shard_map/all_gather | solution.py:31
  30.0 20.1 %all-gather.14.cloned.1.call-done = bf16[4,256,512]{2,1,0:T(8,128)(2,1)} async-done(((bf16[1,256,512]{2,1,0:T(8,128)(2,1)}), bf16[4,256,512]{2,1,0:T(8,128)(2,1)}) %all-gather.14.cloned.1.call-update) | async-done | bytes 1048592 | tf_op jit(solution)/shard_map/all_gather | solution.py:31
  50.2 2.2 fusion.25
  52.6 17.3 %all_gather.28 = bf16[8,1,256]{2,1,0:T(2,128)(2,1)S(1)} all-gather(bf16[1,1,256]{2,1,0:T(2,128)(2,1)S(1)} %reshape.1214), channel_id=1, replica_groups=mesh['sp_0'=8,'sp_1'=4,'tp_0'=8,'tp_1'=2] {'sp_0'}, dimensions={0}, use_global_device_ids=true | all-gather | bytes 4608 | tf_op jit(solution)/shard_map/all_gather | solution.py:31
  69.9 0.5 convolution_select_fusion
  70.3 27.7 %all-gather.8.cloned.1.call-done = bf16[8,1,256,512]{3,2,1,0:T(8,128)(2,1)} async-done(((bf16[1,1,256,512]{3,2,1,0:T(8,128)(2,1)}), bf16[8,1,256,512]{3,2,1,0:T(8,128)(2,1)}) %all-gather.8.cloned.1.call-update) | async-done | bytes 2097168 | tf_op jit(solution)/shard_map/all_gather | solution.py:31
  98.0 3.5 fusion.35
  101.6 0.5 multiply_reduce_fusion.1
  102.2 0.7 convolution_convert_fusion.2
  103.0 33.9 %all_to_all.20 = bf16[16,16,2048]{2,1,0:T(8,128)(2,1)S(1)} all-to-all(bf16[16,16,2048]{2,1,0:T(8,128)(2,1)S(1)} %bitcast.272), channel_id=1, replica_groups=mesh['sp_0'=8,'sp_1'=4,'tp_0'=8,'tp_1'=2] {'tp_0','tp_1'}, dimensions={0} | all-to-all | bytes 2097152 | tf_op jit(solution)/shard_map/all_to_all | solution.py:53
  136.9 0.1 convert_reduce_fusion
  137.2 0.7 multiply_convert_fusion
  138.0 0.2 all-gather.12.cloned.1.call-start
  138.4 0.1 eq.50
  138.5 0.1 eq.46
  138.7 1.2 reduce-window.9
  139.8 0.2 slice_reduce_fusion
  140.5 4.1 %broadcast_multiply_fusion = f32[512,16,32]{2,1,0:T(8,128)} fusion(f32[512,32]{1,0:T(8,128)S(1)} %copy.45, f32[512,16]{1,0:T(8,128)S(1)} %fusion.96), kind=kLoop, calls=%fused_computation.17 | loop fusion | flops 262144 | bytes 1146880 | tf_op jit(solution)/shard_map/mul | solution.py:194
  144.6 3.9 %mul.567 = f32[256,2,512]{2,1,0:T(2,128)S(1)} reshape(f32[512,16,32]{2,1,0:T(8,128)} %broadcast_multiply_fusion) | data formatting | bytes 2097152 | tf_op jit(solution)/shard_map/mul | solution.py:194
  148.4 0.8 copy.46
  149.2 4.2 %multiply_reduce_fusion = (f32[256,512]{1,0:T(8,128)}, bf16[256,512]{1,0:T(8,128)(2,1)S(1)}) fusion(f32[256,2,512]{2,1,0:T(2,128)S(1)} %mul.567, f32[256,2]{1,0:T(8,128)} %copy.46), kind=kLoop, calls=%fused_computation.27 | loop fusion | flops 524288 | bytes 1837056 | tf_op jit(solution)/shard_map/reduce_sum | solution.py:216
  153.4 21.1 %all-gather.10.cloned.1.call-done = bf16[256,2048]{1,0:T(8,128)(2,1)} async-done(((bf16[16,2048]{1,0:T(8,128)(2,1)}), bf16[256,2048]{1,0:T(8,128)(2,1)}) %all-gather.10.cloned.1.call-update) | async-done | bytes 1048592 | tf_op jit(solution)/shard_map/all_gather | solution.py:182
  174.5 2.0 convolution_convert_fusion.1
  176.5 1.2 copy.47
  177.6 61.2 %all_to_all.21 = bf16[16,32,2048]{2,0,1:T(8,128)(2,1)S(1)} all-to-all(bf16[16,32,2048]{2,0,1:T(8,128)(2,1)S(1)} %copy.47), channel_id=1, replica_groups=mesh['sp_0'=8,'sp_1'=4,'tp_0'=8,'tp_1'=2] {'sp_0','sp_1'}, dimensions={1} | all-to-all | bytes 4194304 | tf_op jit(solution)/shard_map/all_to_all | solution.py:198
  238.9 1.2 copy.48
  240.0 1.3 copy-done.1
  241.3 1.6 fusion.16
  242.9 4.8 %convolution_convert_fusion = bf16[512,2048]{1,0:T(8,128)(2,1)} fusion(bf16[512,2048]{1,0:T(8,128)(2,1)} %bitcast.277, bf16[1,176,2048]{2,1,0:T(8,128)(2,1)S(1)} %copy-done.13, bf16[1,2048,176]{1,2,0:T(8,128)(2,1)} %param.32, f32[512,176]{0,1:T(8,128)} %fusion.16), kind=kOutput, calls=%fused_computation.12 | convolution fusion | flops 739786752 | bytes 5996544 | tf_op jit(solution)/shard_map/dot_general | solution.py:210
  247.7 54.5 %all_to_all.22 = bf16[16,32,2048]{2,1,0:T(8,128)(2,1)} all-to-all(bf16[16,32,2048]{2,1,0:T(8,128)(2,1)} %bitcast.278), channel_id=1, replica_groups=mesh['sp_0'=8,'sp_1'=4,'tp_0'=8,'tp_1'=2] {'tp_0','tp_1'}, dimensions={0} | all-to-all | bytes 4194304 | tf_op jit(solution)/shard_map/all_to_all | solution.py:53
  302.2 2.0 reduce_sum.72
  304.2 0.2 copy.58
  304.4 0.5 broadcast.665
  304.9 1.4 reduce.8
  306.4 14.6 %all_to_all.23 = bf16[32,2,1024]{2,1,0:T(2,128)(2,1)S(1)} all-to-all(bf16[32,2,1024]{2,1,0:T(2,128)(2,1)S(1)} %reshape.1223), channel_id=1, replica_groups=mesh['sp_0'=8,'sp_1'=4,'tp_0'=8,'tp_1'=2] {'sp_0','sp_1'}, dimensions={0} | all-to-all | bytes 262144 | tf_op jit(solution)/shard_map/all_to_all | solution.py:215
  321.1 2.2 all_gather.33
  323.3 36.7 %all-gather.12.cloned.1.call-done = bf16[16,32,2048]{2,1,0:T(8,128)(2,1)} async-done(((bf16[2,32,2048]{2,1,0:T(8,128)(2,1)}), bf16[16,32,2048]{2,1,0:T(8,128)(2,1)}) %all-gather.12.cloned.1.call-update) | async-done | bytes 2097168 | tf_op jit(solution)/shard_map/all_gather | solution.py:59
  360.0 3.2 fusion.9
  (68 shorter events, 1.5 us)
Async XLA Ops:
  6.5 95.7 %copy-start = (bf16[512,2048]{1,0:T(8,128)(2,1)S(1)}, bf16[512,2048]{1,0:T(8,128)(2,1)}, u32[]{:S(2)}) copy-start(bf16[512,2048]{1,0:T(8,128)(2,1)} %param.27) | copy-start | bytes 6291460
  6.5 2.5 copy-start.7
  6.5 43.6 %all-gather.14.cloned.1.call-start = ((), (), s32[]{:S(2)}) async-start(), calls=%async_computation.7 | async-start | bytes 1310720 | tf_op jit(solution)/shard_map/all_gather | solution.py:31
  16.3 36.2 %copy-start.6 = (bf16[256,256]{1,0:T(8,128)(2,1)S(1)}, bf16[256,256]{1,0:T(8,128)(2,1)}, u32[]{:S(2)}) copy-start(bf16[256,256]{1,0:T(8,128)(2,1)} %param.19) | copy-start | bytes 393220
  17.1 80.9 %all-gather.8.cloned.1.call-start = ((), (), s32[]{:S(2)}) async-start(), calls=%async_computation.4 | async-start | bytes 2359296 | tf_op jit(solution)/shard_map/all_gather | solution.py:31
  52.3 122.2 %all-gather.10.cloned.1.call-start = ((), (), s32[]{:S(2)}) async-start(), calls=%async_computation.5 | async-start | bytes 1114112 | tf_op jit(solution)/shard_map/all_gather | solution.py:182
  98.0 3.5 copy-start.2
  98.0 3.5 copy-start.5
  98.0 4.0 %copy-start.9 = (f32[512]{0:T(512)S(1)}, f32[512]{0:T(512)}, u32[]{:S(2)}) copy-start(f32[512]{0:T(512)} %param.26) | copy-start | bytes 6148
  102.9 34.1 %copy-start.3 = (bf16[16,2048]{1,0:T(8,128)(2,1)S(1)}, bf16[16,2048]{1,0:T(8,128)(2,1)}, u32[]{:S(2)}) copy-start(bf16[16,2048]{1,0:T(8,128)(2,1)} %param.18) | copy-start | bytes 196612
  102.9 34.3 %copy-start.8 = (f32[2048]{0:T(1024)S(1)}, f32[2048]{0:T(1024)}, u32[]{:S(2)}) copy-start(f32[2048]{0:T(1024)} %param.28) | copy-start | bytes 24580
  103.0 35.2 %copy-start.10 = (s32[256,2]{0,1:T(2,128)S(1)}, s32[256,2]{0,1:T(2,128)}, u32[]{:S(2)}) copy-start(s32[256,2]{0,1:T(2,128)} %param.29) | copy-start | bytes 6148
  138.0 222.1 %all-gather.12.cloned.1.call-start = ((), (), s32[]{:S(2)}) async-start(), calls=%async_computation.6 | async-start | bytes 2359296 | tf_op jit(solution)/shard_map/all_gather | solution.py:59
  144.6 3.9 %copy-start.11 = (f32[256,2]{0,1:T(2,128)S(1)}, f32[256,2]{0,1:T(2,128)}, u32[]{:S(2)}) copy-start(f32[256,2]{0,1:T(2,128)} %param.30) | copy-start | bytes 6148
  238.9 2.5 copy-start.12
  240.0 1.3 copy-start.1
  241.3 1.6 copy-start.13
  302.2 57.9 %copy-start.4 = (bf16[16,2048]{1,0:T(8,128)(2,1)S(1)}, bf16[16,2048]{1,0:T(8,128)(2,1)}, u32[]{:S(2)}) copy-start(bf16[16,2048]{1,0:T(8,128)(2,1)} %param.18) | copy-start | bytes 196612
Sparse Core Ops, SparseCore 0:
  17.2 32.9 all-gather.13
  52.5 45.5 all-gather.7
  138.1 36.3 all-gather.9
  323.5 36.5 all-gather.11
where the time goes:
time: 370 us
  blocking collectives  197 us (53%)
  waiting for transfers between devices  106 us (29%)
  matrix products  22.8 us (6%)
  other arithmetic  20.8 us (6%)
  between operations  13.5 us (4%)
  local copies, waits for them, and re-layouts  10.1 us (3%)
    all_to_all x2, blocking collectives, sent_and_summed(): lax.all_to_all(tiles, axis, split_axis=0, concat_axis=0, tiled=True)  88.4 us
    all_to_all x1, blocking collectives, body(): lax.all_to_all(filled.astype(jnp.bfloat16).reshape(capacity, experts, wid...  61.2 us
    all_gather x2, waiting for transfers between devices, carried_in(): lax.all_gather(part.astype(kind), axis)  47.8 us
    all_gather x1, waiting for transfers between devices, gathered_by_axis(): shard = lax.all_gather(shard, axis, axis=dim, tiled=True)  36.7 us
    all_gather x2, blocking collectives, carried_in(): lax.all_gather(part.astype(kind), axis)  30.1 us
    all_gather x1, waiting for transfers between devices, body(): group = lax.all_gather(normed, TP, axis=0, tiled=True)  21.1 us
    all_to_all x1, blocking collectives, body(): lax.all_to_all(expert_token_rows, SP, split_axis=1, concat_axis=1, tiled=...  14.6 us
  transfers between devices with their start and end apart: 4, of which 4 were waited for; matrix products, arithmetic and copies ran while one was open for 4% of the time, Pallas kernels for 0%

commit v1 on v0

--- a/solution.py
+++ b/solution.py
@@ -179,7 +179,8 @@
     )
     midstream = stream_in.astype(jnp.float32) + attended
     normed = root_scale(midstream, feed_gain)
-    group = lax.all_gather(normed, TP, axis=0, tiled=True)
+    stack = jnp.stack([normed] * lax.axis_size(TP))
+    group = jnp.concatenate(lax.all_to_all(stack, TP, 0, 0), axis=0)
     experts = sequence_devices * expert_gate.shape[0]
     capacity = head_devices * max(1, TOP * length // (sequence_devices * head_devices))
     block_slots = capacity // head_devices

time: 370 us -> 362 us (0.978)
  waiting for transfers between devices: 106 us -> 95.7 us
  starting transfers between devices: 0.31 us -> 4.62 us
    all_gather x1 -> x0, waiting for transfers between devices: 21.1 us -> none  [body(): group = lax.all_gather(normed, TP, axis=0, tiled=True)]
    all_to_all x0 -> x1, waiting for transfers between devices: none -> 11 us  [body(): group = jnp.concatenate(lax.all_to_all(stack, TP, 0, 0), axis=0)]
    all_to_all x0 -> x1, starting transfers between devices: none -> 4.35 us  [body(): group = jnp.concatenate(lax.all_to_all(stack, TP, 0, 0), axis=0)]
where the time goes in v1:
time: 362 us
  blocking collectives  194 us (54%)
  waiting for transfers between devices  95.7 us (26%)
  matrix products  22.8 us (6%)
  other arithmetic  20.2 us (6%)
  between operations  13.5 us (4%)
  local copies, waits for them, and re-layouts  11.2 us (3%)
  starting transfers between devices  4.62 us (1%)
    all_to_all x2, blocking collectives, sent_and_summed(): lax.all_to_all(tiles, axis, split_axis=0, concat_axis=0, tiled=True)  88.5 us
    all_to_all x1, blocking collectives, body(): lax.all_to_all(filled.astype(jnp.bfloat16).reshape(capacity, experts, wid...  58.3 us
    all_gather x2, waiting for transfers between devices, carried_in(): lax.all_gather(part.astype(kind), axis)  47.9 us
    all_gather x1, waiting for transfers between devices, gathered_by_axis(): shard = lax.all_gather(shard, axis, axis=dim, tiled=True)  36.7 us
    all_gather x2, blocking collectives, carried_in(): lax.all_gather(part.astype(kind), axis)  30.1 us
    all_to_all x1, blocking collectives, body(): lax.all_to_all(expert_token_rows, SP, split_axis=1, concat_axis=1, tiled=...  14.6 us
    all_to_all x1, waiting for transfers between devices, body(): group = jnp.concatenate(lax.all_to_all(stack, TP, 0, 0), axis=0)  11 us
  transfers between devices with their start and end apart: 4, of which 4 were waited for; matrix products, arithmetic and copies ran while one was open for 4% of the time, Pallas kernels for 0%

profile of v1, /device:TPU:2, one launch (start us, length us, event | category | flops | bytes accessed | tf_op | source)
XLA Modules:
  0.0 361.7 jit_solution(1803744849385457798)
XLA Ops:
  6.5 1.3 fusion.71
  7.8 0.3 reduce_window_sum.28
  8.1 0.9 convert_element_type.550
  9.1 2.6 convolution_bitcast_fusion.1
  11.7 4.6 %while.13 = (s32[]{:T(128)}, f32[1,256,512]{2,1,0:T(8,128)S(1)}, f32[2,1,128,512]{3,2,1,0:T(8,128)}, f32[2,1,256]{2,1,0:T(1,128)S(1)}, f32[2,1,256,512]{3,2,1,0:...) while((s32[]{:T(128)}, f32[1,256,512]{2,1,0:T(8,128)S(1)}, ...), condition=%wide.region_2.3_spmd.clone, body=%wide.region_1.2_spmd.clone.sunk | while | flops 201850880 | bytes 2494568 | solution.py:95
  11.7 1.2 fusion.144
  12.8 1.2 bitcast_add_fusion.2
  14.0 1.1 fusion.144
  15.2 1.2 bitcast_add_fusion.2
  16.3 0.7 convert_element_type.561
  17.2 12.9 %all-gather.2 = bf16[4,1,256]{2,1,0:T(2,128)(2,1)S(1)} all-gather(bf16[1,1,256]{2,1,0:T(2,128)(2,1)S(1)} %reshape.1213), channel_id=2, replica_groups=mesh['sp_0'=8,'sp_1'=4,'tp_0'=8,'tp_1'=2] {'sp_1'}, dimensions={0}, use_global_device_ids=true | all-gather | bytes 2560 | tf_op jit(solution)/shard_map/all_gather | solution.py:31
  30.0 20.1 %all-gather.11.cloned.1.call-done = bf16[4,256,512]{2,1,0:T(8,128)(2,1)} async-done(((bf16[1,256,512]{2,1,0:T(8,128)(2,1)}), bf16[4,256,512]{2,1,0:T(8,128)(2,1)}) %all-gather.11.cloned.1.call-update) | async-done | bytes 1048592 | tf_op jit(solution)/shard_map/all_gather | solution.py:31
  50.2 2.2 fusion.25
  52.5 17.3 %all_gather.25 = bf16[8,1,256]{2,1,0:T(2,128)(2,1)S(1)} all-gather(bf16[1,1,256]{2,1,0:T(2,128)(2,1)S(1)} %reshape.1220), channel_id=1, replica_groups=mesh['sp_0'=8,'sp_1'=4,'tp_0'=8,'tp_1'=2] {'sp_0'}, dimensions={0}, use_global_device_ids=true | all-gather | bytes 4608 | tf_op jit(solution)/shard_map/all_gather | solution.py:31
  69.8 0.5 convolution_select_fusion
  70.3 27.8 %all-gather.7.cloned.1.call-done = bf16[8,1,256,512]{3,2,1,0:T(8,128)(2,1)} async-done(((bf16[1,1,256,512]{3,2,1,0:T(8,128)(2,1)}), bf16[8,1,256,512]{3,2,1,0:T(8,128)(2,1)}) %all-gather.7.cloned.1.call-update) | async-done | bytes 2097168 | tf_op jit(solution)/shard_map/all_gather | solution.py:31
  98.1 3.5 fusion.35
  101.6 0.5 multiply_reduce_fusion.1
  102.3 0.7 convolution_convert_fusion.2
  103.0 34.0 %all_to_all.25 = bf16[16,16,2048]{2,1,0:T(8,128)(2,1)S(1)} all-to-all(bf16[16,16,2048]{2,1,0:T(8,128)(2,1)S(1)} %bitcast.273), channel_id=1, replica_groups=mesh['sp_0'=8,'sp_1'=4,'tp_0'=8,'tp_1'=2] {'tp_0','tp_1'}, dimensions={0} | all-to-all | bytes 2097152 | tf_op jit(solution)/shard_map/all_to_all | solution.py:53
  137.0 0.1 convert_reduce_fusion
  137.4 1.1 stack.2
  138.6 4.4 %all-to-all-start.1 = ((bf16[16,16,2048]{2,1,0:T(8,128)(2,1)}), bf16[16,16,2048]{2,1,0:T(8,128)(2,1)}, u32[]{:S(2)}, u32[]{:S(2)}) async-start(bf16[16,16,2048]{2,1,0:T(8,128)(2,1)} %stack.2), calls=%async_computation.1 | async-start | bytes 2097152 | tf_op jit(solution)/shard_map/all_to_all | solution.py:183
  142.9 0.2 all-gather.9.cloned.1.call-start
  143.3 0.1 eq.50
  143.6 1.2 reduce-window.9
  144.8 0.2 slice_reduce_fusion
  145.4 4.1 %broadcast_multiply_fusion = f32[512,16,32]{2,1,0:T(8,128)} fusion(f32[512,32]{1,0:T(8,128)S(1)} %copy.45, f32[512,16]{1,0:T(8,128)S(1)} %fusion.96), kind=kLoop, calls=%fused_computation.17 | loop fusion | flops 262144 | bytes 1146880 | tf_op jit(solution)/shard_map/mul | solution.py:195
  149.5 3.9 %mul.567 = f32[256,2,512]{2,1,0:T(2,128)S(1)} reshape(f32[512,16,32]{2,1,0:T(8,128)} %broadcast_multiply_fusion) | data formatting | bytes 2097152 | tf_op jit(solution)/shard_map/mul | solution.py:195
  153.4 0.8 copy.46
  154.2 4.2 %multiply_reduce_fusion = (f32[256,512]{1,0:T(8,128)}, bf16[256,512]{1,0:T(8,128)(2,1)S(1)}) fusion(f32[256,2,512]{2,1,0:T(2,128)S(1)} %mul.567, f32[256,2]{1,0:T(8,128)} %copy.46), kind=kLoop, calls=%fused_computation.27 | loop fusion | flops 524288 | bytes 1837056 | tf_op jit(solution)/shard_map/reduce_sum | solution.py:217
  158.3 11.0 %all-to-all-done.1 = bf16[16,16,2048]{2,1,0:T(8,128)(2,1)} async-done(((bf16[16,16,2048]{2,1,0:T(8,128)(2,1)}), bf16[16,16,2048]{2,1,0:T(8,128)(2,1)}, u32[]{:S(2)}, u32[]{:S(2)}) %all-to-all-start.1) | async-done | bytes 1048608 | tf_op jit(solution)/shard_map/all_to_all | solution.py:183
  169.3 2.0 convolution_convert_fusion.1
  171.3 1.2 copy.47
  172.5 58.3 %all_to_all.26 = bf16[16,32,2048]{2,0,1:T(8,128)(2,1)S(1)} all-to-all(bf16[16,32,2048]{2,0,1:T(8,128)(2,1)S(1)} %copy.47), channel_id=1, replica_groups=mesh['sp_0'=8,'sp_1'=4,'tp_0'=8,'tp_1'=2] {'sp_0','sp_1'}, dimensions={1} | all-to-all | bytes 4194304 | tf_op jit(solution)/shard_map/all_to_all | solution.py:199
  230.7 1.2 copy.48
  231.9 1.3 copy-done.1
  233.2 1.6 fusion.16
  234.8 4.8 %convolution_convert_fusion = bf16[512,2048]{1,0:T(8,128)(2,1)} fusion(bf16[512,2048]{1,0:T(8,128)(2,1)} %bitcast.278, bf16[1,176,2048]{2,1,0:T(8,128)(2,1)S(1)} %copy-done.13, bf16[1,2048,176]{1,2,0:T(8,128)(2,1)} %param.32, f32[512,176]{0,1:T(8,128)} %fusion.16), kind=kOutput, calls=%fused_computation.12 | convolution fusion | flops 739786752 | bytes 5996544 | tf_op jit(solution)/shard_map/dot_general | solution.py:211
  239.5 54.5 %all_to_all.27 = bf16[16,32,2048]{2,1,0:T(8,128)(2,1)} all-to-all(bf16[16,32,2048]{2,1,0:T(8,128)(2,1)} %bitcast.279), channel_id=1, replica_groups=mesh['sp_0'=8,'sp_1'=4,'tp_0'=8,'tp_1'=2] {'tp_0','tp_1'}, dimensions={0} | all-to-all | bytes 4194304 | tf_op jit(solution)/shard_map/all_to_all | solution.py:53
  294.1 2.0 reduce_sum.72
  296.1 0.2 copy.58
  296.3 0.5 broadcast.667
  296.8 1.4 reduce.8
  298.3 14.6 %all_to_all.28 = bf16[32,2,1024]{2,1,0:T(2,128)(2,1)S(1)} all-to-all(bf16[32,2,1024]{2,1,0:T(2,128)(2,1)S(1)} %reshape.1229), channel_id=1, replica_groups=mesh['sp_0'=8,'sp_1'=4,'tp_0'=8,'tp_1'=2] {'sp_0','sp_1'}, dimensions={0} | all-to-all | bytes 262144 | tf_op jit(solution)/shard_map/all_to_all | solution.py:216
  313.1 2.2 all_gather.29
  315.3 36.7 %all-gather.9.cloned.1.call-done = bf16[16,32,2048]{2,1,0:T(8,128)(2,1)} async-done(((bf16[2,32,2048]{2,1,0:T(8,128)(2,1)}), bf16[16,32,2048]{2,1,0:T(8,128)(2,1)}) %all-gather.9.cloned.1.call-update) | async-done | bytes 2097168 | tf_op jit(solution)/shard_map/all_gather | solution.py:59
  352.0 3.2 fusion.9
  (68 shorter events, 1.7 us)
Async XLA Ops:
  6.5 95.7 %copy-start = (bf16[512,2048]{1,0:T(8,128)(2,1)S(1)}, bf16[512,2048]{1,0:T(8,128)(2,1)}, u32[]{:S(2)}) copy-start(bf16[512,2048]{1,0:T(8,128)(2,1)} %param.27) | copy-start | bytes 6291460
  6.5 2.5 copy-start.7
  6.5 43.6 %all-gather.11.cloned.1.call-start = ((), (), s32[]{:S(2)}) async-start(), calls=%async_computation.7 | async-start | bytes 1310720 | tf_op jit(solution)/shard_map/all_gather | solution.py:31
  16.3 36.2 %copy-start.6 = (bf16[256,256]{1,0:T(8,128)(2,1)S(1)}, bf16[256,256]{1,0:T(8,128)(2,1)}, u32[]{:S(2)}) copy-start(bf16[256,256]{1,0:T(8,128)(2,1)} %param.19) | copy-start | bytes 393220
  17.1 81.0 %all-gather.7.cloned.1.call-start = ((), (), s32[]{:S(2)}) async-start(), calls=%async_computation.5 | async-start | bytes 2359296 | tf_op jit(solution)/shard_map/all_gather | solution.py:31
  98.1 3.5 copy-start.2
  98.1 3.5 copy-start.5
  98.1 4.0 %copy-start.9 = (f32[512]{0:T(512)S(1)}, f32[512]{0:T(512)}, u32[]{:S(2)}) copy-start(f32[512]{0:T(512)} %param.26) | copy-start | bytes 6148
  103.0 34.1 %copy-start.3 = (bf16[16,2048]{1,0:T(8,128)(2,1)S(1)}, bf16[16,2048]{1,0:T(8,128)(2,1)}, u32[]{:S(2)}) copy-start(bf16[16,2048]{1,0:T(8,128)(2,1)} %param.18) | copy-start | bytes 196612
  103.0 34.3 %copy-start.8 = (f32[2048]{0:T(1024)S(1)}, f32[2048]{0:T(1024)}, u32[]{:S(2)}) copy-start(f32[2048]{0:T(1024)} %param.28) | copy-start | bytes 24580
  137.2 6.0 %copy-start.10 = (s32[256,2]{0,1:T(2,128)S(1)}, s32[256,2]{0,1:T(2,128)}, u32[]{:S(2)}) copy-start(s32[256,2]{0,1:T(2,128)} %param.29) | copy-start | bytes 6148
  138.6 30.8 %all-to-all-start.1 = ((bf16[16,16,2048]{2,1,0:T(8,128)(2,1)}), bf16[16,16,2048]{2,1,0:T(8,128)(2,1)}, u32[]{:S(2)}, u32[]{:S(2)}) async-start(bf16[16,16,2048]{2,1,0:T(8,128)(2,1)} %stack.2), calls=%async_computation.1 | async-start | bytes 2097152 | tf_op jit(solution)/shard_map/all_to_all | solution.py:183
  142.9 209.0 %all-gather.9.cloned.1.call-start = ((), (), s32[]{:S(2)}) async-start(), calls=%async_computation.6 | async-start | bytes 2359296 | tf_op jit(solution)/shard_map/all_gather | solution.py:59
  149.5 3.9 %copy-start.11 = (f32[256,2]{0,1:T(2,128)S(1)}, f32[256,2]{0,1:T(2,128)}, u32[]{:S(2)}) copy-start(f32[256,2]{0,1:T(2,128)} %param.30) | copy-start | bytes 6148
  230.7 2.5 copy-start.12
  231.9 1.3 copy-start.1
  233.2 1.6 copy-start.13
  294.1 57.9 %copy-start.4 = (bf16[16,2048]{1,0:T(8,128)(2,1)S(1)}, bf16[16,2048]{1,0:T(8,128)(2,1)}, u32[]{:S(2)}) copy-start(bf16[16,2048]{1,0:T(8,128)(2,1)} %param.18) | copy-start | bytes 196612
Sparse Core Ops, SparseCore 0:
  17.2 32.9 all-gather.10
  52.5 45.5 all-gather.6
  315.4 36.5 all-gather.8
